TPU v7x, 32 devices: a whole 2x2x4 slice. The times are simulated.
32 devices in a mesh: fs: 4 (over y, x), tp: 8 (over z, core).
Axes of the slice: x: 2, y: 2, z: 4, core: 2. Of those that a mesh axis runs over, the one named last changes fastest.
Arguments:
- tokens: bfloat16 [4096, 2048], P(('fs', 'tp')), may hold values from -6 to 6
- norm_gain: float32 [2048], replicated, may hold values from 0.1 to 1.9
- gate_weight: bfloat16 [2048, 5632], P('fs', 'tp'), may hold values from -0.125 to 0.125
- up_weight: bfloat16 [2048, 5632], P('fs', 'tp'), may hold values from -0.125 to 0.125
- down_weight: bfloat16 [5632, 2048], P('tp', 'fs'), may hold values from -0.078125 to 0.078125
Outputs:
- mixed: bfloat16 [4096, 2048], P(('fs', 'tp'))
All inputs are finite; a program needn't handle non-finite values.
Results may differ from a plain program's by a relative error of at most 0.0065.
Values may be sent and summed in bfloat16 or wider, within the bound.
A program may use at most 128 MiB of HBM per device.

v0:
```python
import jax
import jax.numpy as jnp
from jax import lax
from jax.sharding import PartitionSpec as P

eps_floor = 0.05


def local(tokens, norm_gain, gate_weight, up_weight, down_weight):
    values = tokens.astype(jnp.float32)
    factor = lax.rsqrt(jnp.mean(values * values, axis=-1, keepdims=True) + eps_floor)
    normed = (values * factor * norm_gain).astype(jnp.bfloat16)
    local_ff = gate_weight.shape[1]
    group = lax.all_gather(normed, "tp", axis=0, tiled=True)
    joined = jnp.concatenate(
        (
            lax.all_gather(gate_weight, "fs", axis=0, tiled=True),
            lax.all_gather(up_weight, "fs", axis=0, tiled=True),
        ),
        axis=1,
    )
    product = jnp.dot(group, joined, preferred_element_type=jnp.float32)
    hidden = (jax.nn.silu(product[:, :local_ff]) * product[:, local_ff:]).astype(jnp.bfloat16)
    down_local = lax.all_gather(down_weight, "fs", axis=1, tiled=True)
    mixed = lax.psum_scatter(
        jnp.dot(hidden, down_local, preferred_element_type=jnp.float32),
        "tp",
        scatter_dimension=0,
        tiled=True,
    )
    return mixed.astype(jnp.bfloat16)


def solution(mesh):
    return jax.shard_map(
        local,
        mesh=mesh,
        in_specs=(P(("fs", "tp"), None), P(), P("fs", "tp"), P("fs", "tp"), P("tp", "fs")),
        out_specs=P(("fs", "tp"), None),
        check_vma=False,
    )
```

profile of v0, /device:TPU:0, one launch (start us, length us, event | category | flops | bytes accessed | tf_op | source)
XLA Modules:
  0.0 296.1 jit_solution(4076748041551358290)
XLA Ops:
  6.5 0.0 all-gather.7.cloned.1.call-start
  6.5 0.7 all-gather.7.cloned.1.call-update
  7.3 0.0 all-gather.9.cloned.1.call-start
  7.3 0.7 all-gather.9.cloned.1.call-update
  8.0 0.0 all-gather.5.cloned.1.call-start
  8.1 1.2 fusion.8
  9.3 2.0 fusion.10
  11.3 0.0 all-gather.5.cloned.1.call-update
  11.3 0.0 all-gather.11.cloned.1.call-start
  11.4 0.5 all-gather.11.cloned.1.call-update
  11.9 0.0 reduce-scatter.2.cloned.1.call-start
  12.0 41.5 %all-gather.7.cloned.1.call-done = bf16[2048,704]{0,1:T(8,128)(2,1)} async-done(((bf16[512,704]{0,1:T(8,128)(2,1)}), bf16[2048,704]{0,1:T(8,128)(2,1)}) %all-gather.7.cloned.1.call-update) | async-done | bytes 2883600 | tf_op jit(solution)/shard_map/all_gather | solution.py:17
  53.5 43.4 %all-gather.9.cloned.1.call-done = bf16[2048,704]{0,1:T(8,128)(2,1)} async-done(((bf16[512,704]{0,1:T(8,128)(2,1)}), bf16[2048,704]{0,1:T(8,128)(2,1)}) %all-gather.9.cloned.1.call-update) | async-done | bytes 2883600 | tf_op jit(solution)/shard_map/all_gather | solution.py:18
  96.9 48.5 %all-gather.5.cloned.1.call-done = bf16[1024,2048]{1,0:T(8,128)(2,1)} async-done(((bf16[128,2048]{1,0:T(8,128)(2,1)}), bf16[1024,2048]{1,0:T(8,128)(2,1)}) %all-gather.5.cloned.1.call-update) | async-done | bytes 4194320 | tf_op jit(solution)/shard_map/all_gather | solution.py:14
  145.4 11.8 %fusion = f32[1024,1408]{1,0:T(8,128)} fusion(bf16[1024,2048]{1,0:T(8,128)(2,1)} %all-gather.5.cloned.1.call-done, bf16[2048,704]{0,1:T(8,128)(2,1)} %all-gather.9.cloned.1.call-done, bf16[2048,704]{0,1:T(8,128)(2,1)} %all-gather.7.cloned.1.call-done), kind=kOutput, calls=%fused_computation | convolution fusion | flops 5917114368 | bytes 15728640 | tf_op jit(solution)/shard_map/dot_general | solution.py:22
  157.2 30.2 %all-gather.11.cloned.1.call-done = bf16[704,2048]{1,0:T(8,128)(2,1)} async-done(((bf16[704,512]{1,0:T(8,128)(2,1)}), bf16[704,2048]{1,0:T(8,128)(2,1)}) %all-gather.11.cloned.1.call-update) | async-done | bytes 2883600 | tf_op jit(solution)/shard_map/all_gather | solution.py:24
  187.4 10.4 %fusion.5 = f32[1024,2048]{1,0:T(8,128)} fusion(bf16[704,2048]{1,0:T(8,128)(2,1)} %all-gather.11.cloned.1.call-done, f32[1024,1408]{1,0:T(8,128)} %fusion), kind=kOutput, calls=%fused_computation.6 | convolution fusion | flops 2957115392 | bytes 17563648 | tf_op jit(solution)/shard_map/dot_general | solution.py:26
  197.8 0.0 reduce-scatter.2.cloned.1.call-update
  197.8 89.7 %reduce-scatter.2.cloned.1.call-done = f32[128,2048]{1,0:T(8,128)} async-done(((f32[1024,2048]{1,0:T(8,128)}), f32[128,2048]{1,0:T(8,128)}) %reduce-scatter.2.cloned.1.call-update) | async-done | bytes 1048592 | tf_op jit(solution)/shard_map/reduce_scatter | solution.py:25
  287.5 2.1 convert_element_type.15
  (1 shorter events, 0.0 us)
Async XLA Ops:
  6.5 46.9 %all-gather.7.cloned.1.call-start = ((), (), s32[]{:S(2)}) async-start(), calls=%async_computation.2 | async-start | bytes 3604480 | tf_op jit(solution)/shard_map/all_gather | solution.py:17
  7.3 89.6 %all-gather.9.cloned.1.call-start = ((), (), s32[]{:S(2)}) async-start(), calls=%async_computation.3 | async-start | bytes 3604480 | tf_op jit(solution)/shard_map/all_gather | solution.py:18
  8.0 137.3 %all-gather.5.cloned.1.call-start = ((), (), s32[]{:S(2)}) async-start(), calls=%async_computation.1 | async-start | bytes 4718592 | tf_op jit(solution)/shard_map/all_gather | solution.py:14
  11.3 176.1 %all-gather.11.cloned.1.call-start = ((), (), s32[]{:S(2)}) async-start(), calls=%async_computation.4 | async-start | bytes 3604480 | tf_op jit(solution)/shard_map/all_gather | solution.py:24
  11.9 275.6 %reduce-scatter.2.cloned.1.call-start = ((), (), s32[]{:S(2)}) async-start(), calls=%async_computation.5 | async-start | bytes 9437184 | tf_op jit(solution)/shard_map/reduce_scatter | solution.py:25
Sparse Core Ops, SparseCore 0:
  9.2 44.2 all-gather.6
  55.3 41.5 all-gather.8
  98.5 46.8 all-gather.4
  147.0 40.3 all-gather.10
  198.0 89.5 reduce-scatter.1
where the time goes:
time: 296 us
  waiting for transfers between devices  255 us (86%)
  matrix products  22.2 us (8%)
  between operations  13.1 us (4%)
  other arithmetic  5.35 us (2%)
    reduce_scatter x1, waiting for transfers between devices, local(): lax.psum_scatter(jnp.dot(hidden, down_local, preferred_element_type=jnp.f...  89.7 us
    all_gather x1, waiting for transfers between devices, local(): group = lax.all_gather(normed, 'tp', axis=0, tiled=True)  48.5 us
    all_gather x1, waiting for transfers between devices, local(): lax.all_gather(up_weight, 'fs', axis=0, tiled=True)  43.4 us
    all_gather x1, waiting for transfers between devices, local(): lax.all_gather(gate_weight, 'fs', axis=0, tiled=True)  41.5 us
    all_gather x1, waiting for transfers between devices, local(): down_local = lax.all_gather(down_weight, 'fs', axis=1, tiled=True)  30.2 us
    dot_general x1, matrix products, local(): product = jnp.dot(group, joined, preferred_element_type=jnp.float32)  11.8 us
    dot_general x1, matrix products, local(): jnp.dot(hidden, down_local, preferred_element_type=jnp.float32)  10.4 us
  transfers between devices with their start and end apart: 5, of which 5 were waited for; matrix products, arithmetic and copies ran while one was open for 5% of the time, Pallas kernels for 0%

commit v1 on v0

--- a/solution.py
+++ b/solution.py
@@ -4,6 +4,16 @@
 from jax.sharding import PartitionSpec as P
 
 eps_floor = 0.05
+
+
+def gather_by_hops(x, name, dim):
+    size = lax.axis_size(name)
+    held, tiles = (x, [x])
+    for _ in range(size - 1):
+        held = lax.ppermute(held, name, [(i, (i + 1) % size) for i in range(size)])
+        tiles.insert(0, held)
+    line = jnp.concatenate(tiles, axis=dim)
+    return jnp.roll(line, (lax.axis_index(name) + 1) * x.shape[dim], axis=dim)
 
 
 def local(tokens, norm_gain, gate_weight, up_weight, down_weight):
@@ -21,7 +31,7 @@
     )
     product = jnp.dot(group, joined, preferred_element_type=jnp.float32)
     hidden = (jax.nn.silu(product[:, :local_ff]) * product[:, local_ff:]).astype(jnp.bfloat16)
-    down_local = lax.all_gather(down_weight, "fs", axis=1, tiled=True)
+    down_local = gather_by_hops(down_weight, "fs", 1)
     mixed = lax.psum_scatter(
         jnp.dot(hidden, down_local, preferred_element_type=jnp.float32),
         "tp",

time: 296 us -> 284 us (0.959)
  waiting for transfers between devices: 255 us -> 234 us
  local copies, waits for them, and re-layouts: 0 us -> 8.03 us
  starting transfers between devices: 0.16 us -> 4.87 us
  matrix products: 22.2 us -> 18.4 us
    ppermute x0 -> x3, waiting for transfers between devices: none -> 73.6 us  [gather_by_hops(): held = lax.ppermute(held, name, [(i, (i + 1) % size) for i in range(size)])]
    all_gather x1, waiting for transfers between devices: 41.5 us -> 0.01 us  [local(): lax.all_gather(gate_weight, 'fs', axis=0, tiled=True)]
    all_gather x1 -> x0, waiting for transfers between devices: 30.2 us -> none  [local(): down_local = lax.all_gather(down_weight, 'fs', axis=1, tiled=True)]
    all_gather x1, waiting for transfers between devices: 43.4 us -> 21.9 us  [local(): lax.all_gather(up_weight, 'fs', axis=0, tiled=True)]
    unnamed x0 -> x9, local copies, waits for them, and re-layouts: none -> 7.05 us
    ppermute x0 -> x3, starting transfers between devices: none -> 4.75 us  [gather_by_hops(): held = lax.ppermute(held, name, [(i, (i + 1) % size) for i in range(size)])]
  transfers between devices with their start and end apart: 5 -> 7, of which waited for: 5 -> 6; matrix products, arithmetic and copies ran while one was open for 5% -> 4% of each run, Pallas kernels for 0% -> 0%
where the time goes in v1:
time: 284 us
  waiting for transfers between devices  234 us (82%)
  matrix products  18.4 us (6%)
  between operations  13.1 us (5%)
  local copies, waits for them, and re-layouts  8.03 us (3%)
  other arithmetic  5.35 us (2%)
  starting transfers between devices  4.87 us (2%)
    reduce_scatter x1, waiting for transfers between devices, local(): lax.psum_scatter(jnp.dot(hidden, down_local, preferred_element_type=jnp.f...  88.5 us
    ppermute x3, waiting for transfers between devices, gather_by_hops(): held = lax.ppermute(held, name, [(i, (i + 1) % size) for i in range(size)])  73.6 us
    all_gather x1, waiting for transfers between devices, local(): group = lax.all_gather(normed, 'tp', axis=0, tiled=True)  48.5 us
    all_gather x1, waiting for transfers between devices, local(): lax.all_gather(up_weight, 'fs', axis=0, tiled=True)  21.9 us
    dot_general x1, matrix products, local(): product = jnp.dot(group, joined, preferred_element_type=jnp.float32)  10.8 us
    dot_general x1, matrix products, local(): jnp.dot(hidden, down_local, preferred_element_type=jnp.float32)  7.69 us
    unnamed x9, local copies, waits for them, and re-layouts  7.05 us
  transfers between devices with their start and end apart: 7, of which 6 were waited for; matrix products, arithmetic and copies ran while one was open for 4% of the time, Pallas kernels for 0%

profile of v1, /device:TPU:0, one launch (start us, length us, event | category | flops | bytes accessed | tf_op | source)
XLA Modules:
  0.0 283.8 jit_solution(17503648726439948337)
XLA Ops:
  6.5 0.7 all-gather.6.cloned.1.call-update
  7.3 0.7 all-gather.8.cloned.1.call-update
  8.1 1.2 fusion.9
  9.3 2.0 fusion.11
  11.4 3.0 %collective-permute-start = (bf16[704,512]{1,0:T(8,128)(2,1)}, bf16[704,512]{1,0:T(8,128)(2,1)S(1)}, u32[]{:S(2)}, u32[]{:S(2)}) collective-permute-start(bf16[704,512]{1,0:T(8,128)(2,1)} %param.9), channel_id=1, source_target_pairs={{0,8},{8,16},{16,24},{24,0},{1,9},{9,17},{17,25},{25,1},{2,10},{10... | collective-permute-start | bytes 2162696 | tf_op jit(solution)/shard_map/ppermute | solution.py:13
  14.4 25.0 %collective-permute-done = bf16[704,512]{1,0:T(8,128)(2,1)S(1)} collective-permute-done((bf16[704,512]{1,0:T(8,128)(2,1)}, bf16[704,512]{1,0:T(8,128)(2,1)S(1)}, u32[]{:S(2)}, u32[]{:S(2)}) %collective-permute-start) | collective-permute-done | bytes 720928 | tf_op jit(solution)/shard_map/ppermute | solution.py:13
  39.4 0.8 collective-permute-start.1
  40.2 31.1 %collective-permute-done.1 = bf16[704,512]{1,0:T(8,128)(2,1)S(1)} collective-permute-done((bf16[704,512]{1,0:T(8,128)(2,1)S(1)}, bf16[704,512]{1,0:T(8,128)(2,1)S(1)}, u32[]{:S(2)}, u32[]{:S(2)}) %collective-permute-start.1) | collective-permute-done | bytes 720928 | tf_op jit(solution)/shard_map/ppermute | solution.py:13
  71.3 0.9 collective-permute-start.2
  72.2 17.5 %collective-permute-done.2 = bf16[704,512]{1,0:T(8,128)(2,1)S(1)} collective-permute-done((bf16[704,512]{1,0:T(8,128)(2,1)S(1)}, bf16[704,512]{1,0:T(8,128)(2,1)S(1)}, u32[]{:S(2)}, u32[]{:S(2)}) %collective-permute-start.2) | collective-permute-done | bytes 720928 | tf_op jit(solution)/shard_map/ppermute | solution.py:13
  89.8 1.0 constant_dynamic-update-slice_fusion.7
  90.8 1.0 constant_dynamic-update-slice_fusion.6
  91.8 1.0 constant_dynamic-update-slice_fusion.5
  92.7 1.0 constant_dynamic-update-slice_fusion.4
  93.8 1.0 constant_dynamic-update-slice_fusion.3
  94.8 1.1 constant_dynamic-update-slice_fusion.2
  95.9 1.0 constant_dynamic-update-slice_fusion.1
  96.9 1.0 constant_dynamic-update-slice_fusion
  97.8 21.9 %all-gather.8.cloned.1.call-done = bf16[2048,704]{0,1:T(8,128)(2,1)} async-done(((bf16[512,704]{0,1:T(8,128)(2,1)}), bf16[2048,704]{0,1:T(8,128)(2,1)}) %all-gather.8.cloned.1.call-update) | async-done | bytes 2883600 | tf_op jit(solution)/shard_map/all_gather | solution.py:28
  119.7 48.5 %all-gather.4.cloned.1.call-done = bf16[1024,2048]{1,0:T(8,128)(2,1)} async-done(((bf16[128,2048]{1,0:T(8,128)(2,1)}), bf16[1024,2048]{1,0:T(8,128)(2,1)}) %all-gather.4.cloned.1.call-update) | async-done | bytes 4194320 | tf_op jit(solution)/shard_map/all_gather | solution.py:24
  168.2 10.8 %fusion = f32[1024,1408]{1,0:T(8,128)S(1)} fusion(bf16[1024,2048]{1,0:T(8,128)(2,1)} %all-gather.4.cloned.1.call-done, bf16[2048,704]{0,1:T(8,128)(2,1)} %all-gather.8.cloned.1.call-done, bf16[2048,704]{0,1:T(8,128)(2,1)} %all-gather.6.cloned.1.call-done), kind=kOutput, calls=%fused_computation | convolution fusion | flops 5917114368 | bytes 15728640 | tf_op jit(solution)/shard_map/dot_general | solution.py:32
  179.0 7.7 %fusion.5 = f32[1024,2048]{1,0:T(8,128)} fusion(bf16[704,4096]{1,0:T(8,128)(2,1)} %constant_dynamic-update-slice_fusion, s32[]{:T(128)S(6)} %select_n.14, f32[1024,1408]{1,0:T(8,128)S(1)} %fusion), kind=kOutput, calls=%fused_computation.6 | convolution fusion | flops 2957115392 | bytes 17563652 | tf_op jit(solution)/shard_map/dot_general | solution.py:36
  186.7 88.5 %reduce-scatter.2.cloned.1.call-done = f32[128,2048]{1,0:T(8,128)} async-done(((f32[1024,2048]{1,0:T(8,128)}), f32[128,2048]{1,0:T(8,128)}) %reduce-scatter.2.cloned.1.call-update) | async-done | bytes 1048592 | tf_op jit(solution)/shard_map/reduce_scatter | solution.py:35
  275.2 2.1 convert_element_type.15
  (10 shorter events, 0.2 us)
Async XLA Ops:
  6.5 86.2 %copy-start = (bf16[704,512]{1,0:T(8,128)(2,1)S(1)}, bf16[704,512]{1,0:T(8,128)(2,1)}, u32[]{:S(2)}) copy-start(bf16[704,512]{1,0:T(8,128)(2,1)} %param.9) | copy-start | bytes 2162692
  6.5 91.3 %all-gather.6.cloned.1.call-start = ((), (), s32[]{:S(2)}) async-start(), calls=%async_computation.2 | async-start | bytes 3604480 | tf_op jit(solution)/shard_map/all_gather | solution.py:27
  7.3 112.4 %all-gather.8.cloned.1.call-start = ((), (), s32[]{:S(2)}) async-start(), calls=%async_computation.3 | async-start | bytes 3604480 | tf_op jit(solution)/shard_map/all_gather | solution.py:28
  8.0 160.2 %all-gather.4.cloned.1.call-start = ((), (), s32[]{:S(2)}) async-start(), calls=%async_computation.1 | async-start | bytes 4718592 | tf_op jit(solution)/shard_map/all_gather | solution.py:24
  11.3 263.8 %reduce-scatter.2.cloned.1.call-start = ((), (), s32[]{:S(2)}) async-start(), calls=%async_computation.4 | async-start | bytes 9437184 | tf_op jit(solution)/shard_map/reduce_scatter | solution.py:35
  11.4 28.0 %collective-permute-start = (bf16[704,512]{1,0:T(8,128)(2,1)}, bf16[704,512]{1,0:T(8,128)(2,1)S(1)}, u32[]{:S(2)}, u32[]{:S(2)}) collective-permute-start(bf16[704,512]{1,0:T(8,128)(2,1)} %param.9), channel_id=1, source_target_pairs={{0,8},{8,16},{16,24},{24,0},{1,9},{9,17},{17,25},{25,1},{2,10},{10... | collective-permute-start | bytes 2162696 | tf_op jit(solution)/shard_map/ppermute | solution.py:13
  39.4 31.9 %collective-permute-start.1 = (bf16[704,512]{1,0:T(8,128)(2,1)S(1)}, bf16[704,512]{1,0:T(8,128)(2,1)S(1)}, u32[]{:S(2)}, u32[]{:S(2)}) collective-permute-start(bf16[704,512]{1,0:T(8,128)(2,1)S(1)} %collective-permute-done), channel_id=1, source_target_pairs={{0,8},{8,16},{16,24},{24,0},{1,9},{9,17},{17,25},{25,1},{2,10},{10... | collective-permute-start | bytes 2162696 | tf_op jit(solution)/shard_map/ppermute | solution.py:13
  71.3 18.5 %collective-permute-start.2 = (bf16[704,512]{1,0:T(8,128)(2,1)S(1)}, bf16[704,512]{1,0:T(8,128)(2,1)S(1)}, u32[]{:S(2)}, u32[]{:S(2)}) collective-permute-start(bf16[704,512]{1,0:T(8,128)(2,1)S(1)} %collective-permute-done.1), channel_id=1, source_target_pairs={{0,8},{8,16},{16,24},{24,0},{1,9},{9,17},{17,25},{25,1},{2,10},{10... | collective-permute-start | bytes 2162696 | tf_op jit(solution)/shard_map/ppermute | solution.py:13
Sparse Core Ops, SparseCore 0:
  9.2 65.8 all-gather.5
  76.8 42.8 all-gather.7
  121.3 46.8 all-gather.3
  186.8 88.3 reduce-scatter.1
